TPU v7x, 512 devices: a whole 4x8x8 slice. The times are simulated.
512 devices in a mesh: sp: 32 (over z, x), tp: 16 (over y, core).
Axes of the slice: x: 4, y: 8, z: 8, core: 2. Of those that a mesh axis runs over, the one named last changes fastest.
Arguments:
- target_rows: bfloat16 [2048, 2048], P(('sp', 'tp')), may hold values from -6 to 6
- source_rows: bfloat16 [8192, 2048], P(('sp', 'tp')), may hold values from -6 to 6
- norm_gain: bfloat16 [2048], replicated, may hold values from 0.099609375 to 1.8984375
- query_weight: bfloat16 [2048, 4096], P(None, 'tp'), may hold values from -0.125 to 0.125
- key_weight: bfloat16 [2048, 4096], P(None, 'tp'), may hold values from -0.125 to 0.125
- value_weight: bfloat16 [2048, 4096], P(None, 'tp'), may hold values from -0.125 to 0.125
- output_weight: bfloat16 [4096, 2048], P('tp'), may hold values from -0.09375 to 0.09375
- saved_output: bfloat16 [2048, 4096], P('sp', 'tp'), may hold values from -3 to 3
- norm_offset: bfloat16 [2048, 16], P('sp', 'tp'), may hold values from 0.25 to 1.25
- output_grad: bfloat16 [2048, 2048], P(('sp', 'tp')), may hold values from -192 to 192
Outputs:
- target_grad: float32 [2048, 2048], P(('sp', 'tp'))
- source_grad: float32 [8192, 2048], P(('sp', 'tp'))
- query_weight_grad: float32 [2048, 4096], P('sp', 'tp')
All inputs are finite; a program needn't handle non-finite values.
Results may differ from a plain program's by a relative error of at most 0.033.
Values may be sent and summed in bfloat16 or wider, within the bound.
A program may use at most 64 MiB of HBM per device.

v0:
```python
import math
import jax
import jax.numpy as jnp
from jax import lax
from jax.sharding import Mesh
from jax.sharding import PartitionSpec as P

HEAD_DIM = 256
SP = ("sp_0", "sp_1")
SP_TP = ("sp_0", "sp_1", "tp")
EPSILON = 1e-06


def from_everyone(shard, axis):
    copies = jnp.broadcast_to(shard, (lax.axis_size(axis), *shard.shape))
    return lax.all_to_all(copies, axis, split_axis=0, concat_axis=0, tiled=True)


def in_order(parts, dim):
    parts = jnp.moveaxis(parts, 0, dim)
    dims = parts.shape
    return parts.reshape(*dims[:dim], dims[dim] * dims[dim + 1], *dims[dim + 2 :])


def gathered_copies(shard, axis, dim):
    parts = from_everyone(shard, axis)
    return in_order(parts, dim)


def side_by_side(arrays, axis, dim, along):
    widths = [math.prod(a.shape[along:]) for a in arrays]
    both = jnp.concatenate(
        [a.reshape(*a.shape[:along], w) for a, w in zip(arrays, widths)], axis=along
    )
    whole = lax.all_gather(both, axis, axis=dim, tiled=True)
    parts = jnp.split(whole, [sum(widths[:k]) for k in range(1, len(widths))], axis=along)
    return tuple((b.reshape(*whole.shape[:along], *a.shape[along:]) for a, b in zip(arrays, parts)))


def sum_by_axis(shard, axes, dim):
    if not axes:
        return shard
    nearer = lax.psum_scatter(shard, axes[0], scatter_dimension=dim, tiled=True)
    return sum_by_axis(nearer, axes[1:], dim)


def cut_along(shard, dim, size):
    before, after = (shard.shape[:dim], shard.shape[dim + 1 :])
    return jnp.moveaxis(shard.reshape(*before, size, -1, *after), dim, 0)


def sum_at_owner(shard, axis, dim):
    size = lax.axis_size(axis)
    parts = lax.all_to_all(cut_along(shard, dim, size), axis, 0, 0, tiled=True)
    return jnp.sum(parts.astype(jnp.float32), axis=0)


def sum_at_owner_2(shard, axis, dim):
    size = lax.axis_size(axis)
    parts = lax.all_to_all(cut_along(shard, dim, size), axis, 0, 0, tiled=True)
    return jnp.sum(parts, axis=0)


def contract_last(left, right):
    return lax.dot_general(
        left, right, (((1,), (1,)), ((), ())), preferred_element_type=jnp.float32
    )


def attention_weights(
    query_rows, head_gradient, offsets, deltas, key_row_block, value_row_block, shift_base
):
    score_scale = HEAD_DIM ** (-0.5)
    score_matrix = jnp.einsum(
        "rfo,kfo->frk", query_rows, key_row_block, preferred_element_type=jnp.float32
    )
    shifts = jnp.transpose(shift_base + offsets.astype(jnp.float32))[:, :, None]
    prob_rows = jnp.exp(score_matrix * score_scale - shifts)
    prob_grad = jnp.einsum(
        "rfo,kfo->frk", head_gradient, value_row_block, preferred_element_type=jnp.float32
    )
    score_grad = (
        prob_rows
        * (prob_grad - jnp.transpose(deltas.astype(jnp.float32))[:, :, None])
        * score_scale
    )
    return (prob_rows.astype(jnp.bfloat16), score_grad.astype(jnp.bfloat16))


def body(
    target_rows,
    source_rows,
    norm_gain,
    query_weight,
    key_weight,
    value_weight,
    output_weight,
    saved_output,
    norm_offset,
    output_grad,
):
    tp_count = lax.axis_size("tp")
    sp_count = lax.axis_size(SP)
    query_width = query_weight.shape[1]
    local_heads = query_width // HEAD_DIM
    target_count = saved_output.shape[0]
    source_count = source_rows.shape[0] * tp_count
    shift_base = math.log(source_count * sp_count)
    target_float = target_rows.astype(jnp.float32)
    gain_float = norm_gain.astype(jnp.float32)
    inverse = lax.rsqrt(jnp.mean(target_float * target_float, axis=1, keepdims=True) + EPSILON)
    normed = (target_float * inverse * gain_float).astype(jnp.bfloat16)
    slice_share = lax.all_gather(jnp.stack([normed, output_grad]), "tp", axis=1, tiled=True)
    query_part = jnp.dot(slice_share[0], query_weight, preferred_element_type=jnp.float32).astype(
        jnp.bfloat16
    )
    grad_part = contract_last(slice_share[1], output_weight).astype(jnp.bfloat16)
    joined = jnp.concatenate([query_part, grad_part, slice_share[0]], axis=1)
    query_rows = joined[:, :query_width].reshape(target_count, local_heads, HEAD_DIM)
    head_gradient = joined[:, query_width : 2 * query_width].reshape(
        target_count, local_heads, HEAD_DIM
    )
    normed_all = joined[:, 2 * query_width :]
    saved_heads = saved_output.reshape(target_count, local_heads, HEAD_DIM)
    deltas = jnp.sum(
        head_gradient.astype(jnp.float32) * saved_heads.astype(jnp.float32), axis=2
    ).astype(jnp.bfloat16)
    slice_share = gathered_copies(source_rows, "tp", 0)
    key_part = jnp.dot(slice_share, key_weight, preferred_element_type=jnp.float32).astype(
        jnp.bfloat16
    )
    value_part = jnp.dot(slice_share, value_weight, preferred_element_type=jnp.float32).astype(
        jnp.bfloat16
    )
    projected = jnp.concatenate([key_part, value_part], axis=1)
    key_row_block = projected[:, :query_width].reshape(source_count, local_heads, HEAD_DIM)
    value_row_block = projected[:, query_width:].reshape(source_count, local_heads, HEAD_DIM)
    slice_share = side_by_side((query_rows, head_gradient, norm_offset, deltas), SP, 0, 2)
    probability_rounded, score_rounded = attention_weights(
        slice_share[0],
        slice_share[1],
        slice_share[2],
        slice_share[3],
        key_row_block,
        value_row_block,
        shift_base,
    )
    key_total = jnp.einsum(
        "wcu,cwp->uwp", score_rounded, slice_share[0], preferred_element_type=jnp.float32
    )
    value_total = jnp.einsum(
        "wcu,cwp->uwp", probability_rounded, slice_share[1], preferred_element_type=jnp.float32
    )
    key_total, value_total, score_rounded = (key_total, value_total, score_rounded)
    query_term = jnp.einsum(
        "tje,etq->jtq", score_rounded, key_row_block, preferred_element_type=jnp.float32
    )
    query_grad = sum_by_axis(query_term.astype(jnp.bfloat16), SP, 0).astype(jnp.float32)
    query_flat = query_grad.astype(jnp.bfloat16).reshape(target_count, query_width)
    normed_grad = sum_at_owner(
        contract_last(query_flat, query_weight).astype(jnp.bfloat16), "tp", 0
    )
    scaled = normed_grad * gain_float
    target_grad = inverse * scaled - target_float * inverse**3 * jnp.mean(
        scaled * target_float, axis=1, keepdims=True
    )
    key_flat = key_total.astype(jnp.bfloat16).reshape(source_count, query_width)
    value_flat = value_total.astype(jnp.bfloat16).reshape(source_count, query_width)
    key_part = contract_last(key_flat, key_weight)
    value_part = contract_last(value_flat, value_weight)
    source_grad = sum_at_owner((key_part + value_part).astype(jnp.bfloat16), "tp", 0)
    weight_grad = sum_at_owner_2(
        lax.dot_general(
            normed_all, query_flat, (((0,), (0,)), ((), ())), preferred_element_type=jnp.float32
        ),
        SP,
        0,
    )
    return (target_grad, source_grad, weight_grad)


def solution(mesh):
    split = Mesh(mesh.devices.reshape(8, 4, mesh.shape["tp"]), ("sp_0", "sp_1", "tp"))
    placed = (
        P(SP_TP, None),
        P(SP_TP, None),
        P(),
        P(None, "tp"),
        P(None, "tp"),
        P(None, "tp"),
        P("tp", None),
        P(SP, "tp"),
        P(SP, "tp"),
        P(SP_TP, None),
    )
    return jax.shard_map(
        body,
        mesh=split,
        in_specs=placed,
        out_specs=(P(SP_TP, None), P(SP_TP, None), P(SP, "tp")),
        check_vma=False,
    )
```

profile of v0, /device:TPU:3, one launch (start us, length us, event | category | flops | bytes accessed | tf_op | source)
XLA Modules:
  0.0 286.7 jit_solution(7998154061447127349)
XLA Ops:
  7.2 0.0 copy-start
  7.2 0.0 all-gather.2.cloned.1.call-start
  7.2 1.0 fusion.13
  8.2 0.7 convert_element_type.117
  8.9 0.8 fusion.21
  9.7 0.0 copy-start.3
  9.7 0.8 pad_maximum_fusion.1
  10.6 0.8 copy.28
  11.4 19.5 %all_gather.6 = bf16[2,64,2048]{2,0,1:T(2,128)(2,1)S(1)} all-gather(bf16[2,4,2048]{2,0,1:T(2,128)(2,1)S(1)} %copy.25), channel_id=1, replica_groups=mesh['sp_0'=8,'sp_1'=4,'tp'=16] {'tp'}, dimensions={1}, use_global_device_ids=true | all-gather | bytes 557056 | tf_op jit(solution)/shard_map/all_gather | solution.py:113
  30.9 1.6 fusion.22
  32.5 0.6 multiply_reduce_fusion
  33.1 0.1 copy.29
  33.2 0.0 copy-start.1
  33.2 1.5 fusion.10
  34.7 0.7 pad_maximum_fusion
  35.4 0.0 all-gather.2.cloned.1.call-update
  35.4 0.0 reduce-scatter.5.cloned.1.call-start
  35.5 0.1 broadcast_in_dim.2
  35.6 32.7 %all_to_all.20 = bf16[16,16,2048]{2,1,0:T(8,128)(2,1)S(1)} all-to-all(bf16[16,16,2048]{2,1,0:T(8,128)(2,1)S(1)} %broadcast_in_dim.2), channel_id=1, replica_groups=mesh['sp_0'=8,'sp_1'=4,'tp'=16] {'tp'}, dimensions={0} | all-to-all | bytes 2097152 | tf_op jit(solution)/shard_map/all_to_all | solution.py:16
  68.3 0.4 convolution_convert_fusion.5
  68.8 47.4 %all-gather.2.cloned.1.call-done = bf16[2048,1,514]{2,0,1:T(8,128)(2,1)} async-done(((bf16[64,1,514]{2,0,1:T(8,128)(2,1)}), bf16[2048,1,514]{2,0,1:T(8,128)(2,1)}) %all-gather.2.cloned.1.call-update) | async-done | bytes 2105360 | tf_op jit(solution)/shard_map/all_gather | solution.py:35
  116.2 1.9 convert_reduce_fusion.1
  118.0 3.1 %fusion.3 = f32[2048,256]{1,0:T(8,128)} fusion(bf16[256,256]{1,0:T(8,128)(2,1)S(1)} %convolution_convert_fusion.5, f32[2048]{0:T(1024)S(1)} %get-tuple-element.4, bf16[2048,1,514]{2,0,1:T(8,128)(2,1)} %all-gather.2.cloned.1.call-done), kind=kOutput, calls=%fused_computation.6 | convolution fusion | flops 269484032 | bytes 3284992 | tf_op jit(solution)/shard_map/rfo,kfo->frk/dot_general | solution.py:74
  121.1 3.3 %fusion.5 = bf16[2048,256]{1,0:T(8,128)(2,1)S(1)} fusion(f32[2048,256]{1,0:T(8,128)} %fusion.3, bf16[256,2048]{1,0:T(8,128)(2,1)S(1)} %bitcast.80, bf16[2048,256]{1,0:T(8,128)(2,1)S(1)} %copy-done, f32[2048]{0:T(1024)S(1)} %get-tuple-element.3, bf16[2048,1,514]{2,0,1:T(8,128)(2,1)} %all-gather.2.cloned.1.call-done), kind=kOutput, calls=%fused_computation.9 | convolution fusion | flops 539033600 | bytes 6299648 | tf_op jit(solution)/shard_map/rfo,kfo->frk/dot_general | solution.py:79
  124.4 0.0 copy-start.2
  124.4 1.6 fusion.6
  126.0 0.0 reduce-scatter.5.cloned.1.call-update
  126.0 4.0 %fusion.8 = f32[256,2048]{1,0:T(8,128)} fusion(bf16[2048,256]{1,0:T(8,128)(2,1)S(1)} %copy-done.2, bf16[2048,256]{1,0:T(8,128)(2,1)S(1)} %fusion.5, bf16[2048,1,514]{2,0,1:T(8,128)(2,1)} %all-gather.2.cloned.1.call-done), kind=kOutput, calls=%fused_computation.18 | convolution fusion | flops 536936448 | bytes 5242880 | tf_op jit(solution)/shard_map/dot_general | solution.py:65
  130.0 4.9 %fusion.4 = bf16[256,2048]{1,0:T(8,128)(2,1)} fusion(f32[256,2048]{1,0:T(8,128)} %fusion.8, bf16[2048,256]{1,0:T(8,128)(2,1)S(1)} %copy-done, f32[2048,256]{1,0:T(8,128)} %fusion.3, bf16[2048,1,514]{2,0,1:T(8,128)(2,1)} %all-gather.2.cloned.1.call-done), kind=kOutput, calls=%fused_computation.7 | convolution fusion | flops 538509312 | bytes 7340032 | tf_op jit(solution)/shard_map/dot_general | solution.py:65
  134.9 11.8 %all-to-all-start.2 = ((bf16[16,16,2048]{2,1,0:T(8,128)(2,1)}), bf16[16,16,2048]{2,1,0:T(8,128)(2,1)S(1)}, u32[]{:S(2)}, u32[]{:S(2)}) async-start(bf16[16,16,2048]{2,1,0:T(8,128)(2,1)} %bitcast.20), calls=%async_computation.3 | async-start | bytes 2097152 | tf_op jit(solution)/shard_map/all_to_all | solution.py:54
  146.7 0.0 reduce-scatter.7.cloned.1.call-start
  146.7 19.3 %reduce-scatter.5.cloned.1.call-done = bf16[256,1,256]{0,2,1:T(8,128)(2,1)} async-done(((bf16[2048,1,256]{0,2,1:T(8,128)(2,1)}), bf16[256,1,256]{0,2,1:T(8,128)(2,1)}) %reduce-scatter.5.cloned.1.call-update) | async-done | bytes 131088 | tf_op jit(solution)/shard_map/reduce_scatter | solution.py:43
  166.0 1.7 copy.36
  167.7 0.0 reduce-scatter.7.cloned.1.call-update
  167.7 26.5 %reduce-scatter.7.cloned.1.call-done = bf16[64,256]{1,0:T(8,128)(2,1)} async-done(((bf16[256,256]{1,0:T(8,128)(2,1)}), bf16[64,256]{1,0:T(8,128)(2,1)}) %reduce-scatter.7.cloned.1.call-update) | async-done | bytes 32784 | tf_op jit(solution)/shard_map/reshape | solution.py:159
  194.2 1.3 convolution_convert_fusion.1
  195.5 0.8 reshape.145
  196.3 9.5 %all-to-all-start.1 = ((bf16[16,4,2048]{2,1,0:T(4,128)(2,1)}), bf16[16,4,2048]{2,1,0:T(4,128)(2,1)S(1)}, u32[]{:S(2)}, u32[]{:S(2)}) async-start(bf16[16,4,2048]{2,1,0:T(4,128)(2,1)} %reshape.145), calls=%async_computation.2 | async-start | bytes 524288 | tf_op jit(solution)/shard_map/all_to_all | solution.py:54
  205.8 1.4 copy.40
  207.2 1.8 fusion.19
  209.0 8.4 %all-to-all-done.1 = bf16[16,4,2048]{2,1,0:T(4,128)(2,1)S(1)} async-done(((bf16[16,4,2048]{2,1,0:T(4,128)(2,1)}), bf16[16,4,2048]{2,1,0:T(4,128)(2,1)S(1)}, u32[]{:S(2)}, u32[]{:S(2)}) %all-to-all-start.1) | async-done | bytes 262176 | tf_op jit(solution)/shard_map/all_to_all | solution.py:54
  217.4 10.3 %all-to-all-start.3 = ((f32[32,64,256]{2,1,0:T(8,128)}), f32[32,64,256]{2,1,0:T(8,128)S(1)}, u32[]{:S(2)}, u32[]{:S(2)}) async-start(f32[32,64,256]{2,1,0:T(8,128)} %fusion.19), calls=%async_computation.4 | async-start | bytes 4194304 | tf_op jit(solution)/shard_map/all_to_all | solution.py:60
  227.6 2.0 convert_reduce_fusion
  229.7 0.1 convert_reduce_fusion.2
  229.8 0.1 fusion.18
  229.9 0.7 fusion.17
  230.6 48.7 %all-to-all-done.3 = f32[32,64,256]{2,1,0:T(8,128)S(1)} async-done(((f32[32,64,256]{2,1,0:T(8,128)}), f32[32,64,256]{2,1,0:T(8,128)S(1)}, u32[]{:S(2)}, u32[]{:S(2)}) %all-to-all-start.3) | async-done | bytes 2097184 | tf_op jit(solution)/shard_map/all_to_all | solution.py:60
  279.4 0.8 reduce_sum.59
  (22 shorter events, 0.1 us)
Async XLA Ops:
  7.2 114.0 %copy-start = (bf16[2048,256]{1,0:T(8,128)(2,1)S(1)}, bf16[2048,256]{1,0:T(8,128)(2,1)}, u32[]{:S(2)}) copy-start(bf16[2048,256]{1,0:T(8,128)(2,1)} %param.15) | copy-start | bytes 3145732
  7.2 25.3 %copy-start.10 = (bf16[64,256]{1,0:T(8,128)(2,1)S(1)}, bf16[64,256]{1,0:T(8,128)(2,1)}, u32[]{:S(2)}) copy-start(bf16[64,256]{1,0:T(8,128)(2,1)} %param.17) | copy-start | bytes 98308
  7.2 25.3 %copy-start.6 = (bf16[256,2048]{1,0:T(8,128)(2,1)S(1)}, bf16[256,2048]{1,0:T(8,128)(2,1)}, u32[]{:S(2)}) copy-start(bf16[256,2048]{1,0:T(8,128)(2,1)} %param.16) | copy-start | bytes 3145732
  7.2 109.0 %all-gather.2.cloned.1.call-start = ((), (), s32[]{:S(2)}) async-start(), calls=%async_computation.6 | async-start | bytes 2703360 | tf_op jit(solution)/shard_map/all_gather | solution.py:35
  9.7 23.5 %copy-start.3 = (bf16[2048,256]{1,0:T(8,128)(2,1)S(1)}, bf16[2048,256]{1,0:T(8,128)(2,1)}, u32[]{:S(2)}) copy-start(bf16[2048,256]{1,0:T(8,128)(2,1)} %param.13) | copy-start | bytes 3145732
  30.9 4.6 %copy-start.9 = (bf16[16,2048]{1,0:T(8,128)(2,1)S(1)}, bf16[16,2048]{1,0:T(8,128)(2,1)}, u32[]{:S(2)}) copy-start(bf16[16,2048]{1,0:T(8,128)(2,1)} %param.11) | copy-start | bytes 196612
  33.2 35.1 %copy-start.1 = (bf16[2048,256]{1,0:T(8,128)(2,1)S(1)}, bf16[2048,256]{1,0:T(8,128)(2,1)}, u32[]{:S(2)}) copy-start(bf16[2048,256]{1,0:T(8,128)(2,1)} %param.14) | copy-start | bytes 3145732
  35.4 130.6 %reduce-scatter.5.cloned.1.call-start = ((), (), s32[]{:S(2)}) async-start(), calls=%async_computation.7 | async-start | bytes 1179648 | tf_op jit(solution)/shard_map/reduce_scatter | solution.py:43
  124.4 1.6 copy-start.2
  134.9 59.3 %copy-start.4 = (bf16[2048,256]{1,0:T(8,128)(2,1)S(1)}, bf16[2048,256]{1,0:T(8,128)(2,1)}, u32[]{:S(2)}) copy-start(bf16[2048,256]{1,0:T(8,128)(2,1)} %param.13) | copy-start | bytes 3145732
  134.9 61.3 %all-to-all-start.2 = ((bf16[16,16,2048]{2,1,0:T(8,128)(2,1)}), bf16[16,16,2048]{2,1,0:T(8,128)(2,1)S(1)}, u32[]{:S(2)}, u32[]{:S(2)}) async-start(bf16[16,16,2048]{2,1,0:T(8,128)(2,1)} %bitcast.20), calls=%async_computation.3 | async-start | bytes 2097152 | tf_op jit(solution)/shard_map/all_to_all | solution.py:54
  146.7 47.5 %reduce-scatter.7.cloned.1.call-start = ((), (), s32[]{:S(2)}) async-start(), calls=%async_computation.8 | async-start | bytes 163840 | tf_op jit(solution)/shard_map/reshape | solution.py:159
  194.2 13.0 %copy-start.8 = (bf16[64,256]{1,0:T(8,128)(2,1)S(1)}, bf16[64,256]{1,0:T(8,128)(2,1)}, u32[]{:S(2)}) copy-start(bf16[64,256]{1,0:T(8,128)(2,1)} %reduce-scatter.7.cloned.1.call-done) | copy-start | bytes 98308
  196.3 12.7 %copy-start.5 = (bf16[16,16,2048]{2,1,0:T(8,128)(2,1)}, bf16[16,16,2048]{2,1,0:T(8,128)(2,1)S(1)}, u32[]{:S(2)}) copy-start(bf16[16,16,2048]{2,1,0:T(8,128)(2,1)S(1)} %all-to-all-done.2) | copy-start | bytes 3145732
  196.3 21.1 %all-to-all-start.1 = ((bf16[16,4,2048]{2,1,0:T(4,128)(2,1)}), bf16[16,4,2048]{2,1,0:T(4,128)(2,1)S(1)}, u32[]{:S(2)}, u32[]{:S(2)}) async-start(bf16[16,4,2048]{2,1,0:T(4,128)(2,1)} %reshape.145), calls=%async_computation.2 | async-start | bytes 524288 | tf_op jit(solution)/shard_map/all_to_all | solution.py:54
  209.0 20.8 %copy-start.7 = (bf16[4,2048]{1,0:T(4,128)(2,1)S(1)}, bf16[4,2048]{1,0:T(4,128)(2,1)}, u32[]{:S(2)}) copy-start(bf16[4,2048]{1,0:T(4,128)(2,1)} %param.10) | copy-start | bytes 49156
  217.4 62.0 %all-to-all-start.3 = ((f32[32,64,256]{2,1,0:T(8,128)}), f32[32,64,256]{2,1,0:T(8,128)S(1)}, u32[]{:S(2)}, u32[]{:S(2)}) async-start(f32[32,64,256]{2,1,0:T(8,128)} %fusion.19), calls=%async_computation.4 | async-start | bytes 4194304 | tf_op jit(solution)/shard_map/all_to_all | solution.py:60
Sparse Core Ops, SparseCore 0:
  35.6 80.5 all-gather.1
  126.1 39.8 reduce-scatter.4
  169.4 24.7 reduce-scatter.6
where the time goes:
time: 287 us
  waiting for transfers between devices  150 us (52%)
  blocking collectives  52.2 us (18%)
  starting transfers between devices  31.6 us (11%)
  matrix products  22.3 us (8%)
  between operations  13.9 us (5%)
  other arithmetic  9.66 us (3%)
  local copies, waits for them, and re-layouts  6.56 us (2%)
    all_to_all x1, waiting for transfers between devices, sum_at_owner_2(): parts = lax.all_to_all(cut_along(shard, dim, size), axis, 0, 0, tiled=True)  48.7 us
    all_gather x1, waiting for transfers between devices, side_by_side(): whole = lax.all_gather(both, axis, axis=dim, tiled=True)  47.4 us
    all_to_all x1, blocking collectives, from_everyone(): return lax.all_to_all(copies, axis, split_axis=0, concat_axis=0, tiled=True)  32.7 us
    reshape x1, waiting for transfers between devices, body(): query_grad.astype(jnp.bfloat16).reshape(target_count, query_width)  26.5 us
    all_to_all x2, starting transfers between devices, sum_at_owner(): parts = lax.all_to_all(cut_along(shard, dim, size), axis, 0, 0, tiled=True)  21.3 us
    all_gather x1, blocking collectives, body(): lax.all_gather(jnp.stack([normed, output_grad]), 'tp', axis=1, tiled=True)  19.5 us
    reduce_scatter x1, waiting for transfers between devices, sum_by_axis(): nearer = lax.psum_scatter(shard, axes[0], scatter_dimension=dim, tiled=True)  19.3 us
    dot_general x4, matrix products, contract_last(): lax.dot_general(left, right, (((1,), (1,)), ((), ())), preferred_element_...  10.7 us
  transfers between devices with their start and end apart: 6, of which 5 were waited for; matrix products, arithmetic and copies ran while one was open for 7% of the time, Pallas kernels for 0%

commit v1 on v0

--- a/solution.py
+++ b/solution.py
@@ -110,7 +110,26 @@
     gain_float = norm_gain.astype(jnp.float32)
     inverse = lax.rsqrt(jnp.mean(target_float * target_float, axis=1, keepdims=True) + EPSILON)
     normed = (target_float * inverse * gain_float).astype(jnp.bfloat16)
-    slice_share = lax.all_gather(jnp.stack([normed, output_grad]), "tp", axis=1, tiled=True)
+    shard_2 = jnp.stack([normed, output_grad])
+    length, here, extent = (lax.axis_size("tp"), lax.axis_index("tp"), shard_2.shape[1])
+    route = [(i, (i + 1) % length) for i in range(length)]
+    backward = [(i, (i - 1) % length) for i in range(length)]
+    slice_share = jnp.zeros(
+        (*shard_2.shape[:1], length * extent, *shard_2.shape[1 + 1 :]), shard_2.dtype
+    )
+    slice_share = lax.dynamic_update_slice_in_dim(slice_share, shard_2, here * extent, axis=1)
+    from_left = from_right = shard_2
+    half = length // 2
+    for step in range(1, half + 1):
+        from_left = lax.ppermute(from_left, "tp", route)
+        slice_share = lax.dynamic_update_slice_in_dim(
+            slice_share, from_left, (here - step) % length * extent, axis=1
+        )
+        if step < length - half:
+            from_right = lax.ppermute(from_right, "tp", backward)
+            slice_share = lax.dynamic_update_slice_in_dim(
+                slice_share, from_right, (here + step) % length * extent, axis=1
+            )
     query_part = jnp.dot(slice_share[0], query_weight, preferred_element_type=jnp.float32).astype(
         jnp.bfloat16
     )

time: 287 us -> 434 us (1.51)
  local copies, waits for them, and re-layouts: 6.56 us -> 134 us
  starting transfers between devices: 31.6 us -> 53.6 us
  blocking collectives: 52.2 us -> 40.6 us
  waiting for transfers between devices: 150 us -> 157 us
    dynamic_update_slice x0 -> x16, local copies, waits for them, and re-layouts: none -> 119 us  [the longest x8 59.9 us: body(): lax.dynamic_update_slice_in_dim(slice_share, from_left, (here - step) % l...]
    ppermute x0 -> x15, starting transfers between devices: none -> 22 us  [the longest x7 13.9 us: body(): from_right = lax.ppermute(from_right, 'tp', backward)]
    all_gather x1 -> x0, blocking collectives: 19.5 us -> none  [body(): lax.all_gather(jnp.stack([normed, output_grad]), 'tp', axis=1, tiled=True)]
    ppermute x0 -> x15, local copies, waits for them, and re-layouts: none -> 10.1 us  [the longest x8 5.77 us: body(): from_left = lax.ppermute(from_left, 'tp', route)]
    all_to_all x1, blocking collectives: 32.7 us -> 40.6 us  [from_everyone(): return lax.all_to_all(copies, axis, split_axis=0, concat_axis=0, tiled=True)]
    ppermute x0 -> x15, waiting for transfers between devices: none -> 6.68 us  [the longest x8 5.44 us: body(): from_left = lax.ppermute(from_left, 'tp', route)]
  transfers between devices with their start and end apart: 6 -> 21, of which waited for: 5 -> 17; matrix products, arithmetic and copies ran while one was open for 7% -> 32% of each run, Pallas kernels for 0% -> 0%
where the time goes in v1:
time: 434 us; the launch traced here: 433 us
  waiting for transfers between devices  157 us (36%)
  local copies, waits for them, and re-layouts  134 us (31%)
  starting transfers between devices  53.6 us (12%)
  blocking collectives  40.6 us (9%)
  matrix products  24 us (6%)
  between operations  14.5 us (3%)
  other arithmetic  9.51 us (2%)
    dynamic_update_slice x8, local copies, waits for them, and re-layouts, body(): lax.dynamic_update_slice_in_dim(slice_share, from_left, (here - step) % l...  59.9 us
    dynamic_update_slice x7, local copies, waits for them, and re-layouts, body(): lax.dynamic_update_slice_in_dim(slice_share, from_right, (here + step) %...  52 us
    all_to_all x1, waiting for transfers between devices, sum_at_owner_2(): parts = lax.all_to_all(cut_along(shard, dim, size), axis, 0, 0, tiled=True)  48.7 us
    all_gather x1, waiting for transfers between devices, side_by_side(): whole = lax.all_gather(both, axis, axis=dim, tiled=True)  46.2 us
    all_to_all x1, blocking collectives, from_everyone(): return lax.all_to_all(copies, axis, split_axis=0, concat_axis=0, tiled=True)  40.6 us
    reshape x1, waiting for transfers between devices, body(): query_grad.astype(jnp.bfloat16).reshape(target_count, query_width)  26.3 us
    all_to_all x2, starting transfers between devices, sum_at_owner(): parts = lax.all_to_all(cut_along(shard, dim, size), axis, 0, 0, tiled=True)  21.2 us
    reduce_scatter x1, waiting for transfers between devices, sum_by_axis(): nearer = lax.psum_scatter(shard, axes[0], scatter_dimension=dim, tiled=True)  19.5 us
  transfers between devices with their start and end apart: 21, of which 17 were waited for; matrix products, arithmetic and copies ran while one was open for 32% of the time, Pallas kernels for 0%

profile of v1, /device:TPU:3, one launch (start us, length us, event | category | flops | bytes accessed | tf_op | source)
XLA Modules:
  0.0 433.0 jit_solution(17305853850601862335)
XLA Ops:
  10.4 1.9 collective-permute-start
  12.3 1.0 collective-permute-done
  13.3 2.3 collective-permute-start.2
  16.6 2.3 collective-permute-start.4
  20.9 1.4 collective-permute-start.6
  22.6 2.2 collective-permute-start.7
  25.9 3.4 collective-permute-start.9
  30.2 3.7 collective-permute-start.11
  34.7 3.7 collective-permute-start.13
  40.9 7.4 %dynamic_update_slice.48 = bf16[2,64,2048]{1,2,0:T(8,128)(2,1)S(1)} dynamic-update-slice(bf16[2,64,2048]{1,2,0:T(8,128)(2,1)S(1)} %broadcast_in_dim.5, bf16[2,4,2048]{1,2,0:T(8,128)(2,1)S(1)} %copy.51, s32[]{:T(128)} %constant.99.clone.1, s32[]{:T(128)S(6)} %select_n.111, s32[]{:T(128)} %constant.99.clone.1) | dynamic-update-slice | bytes 65540 | tf_op jit(solution)/shard_map/dynamic_update_slice | solution.py:120
  48.8 4.1 dynamic_update_slice.49
  53.4 7.4 %dynamic_update_slice.50 = bf16[2,64,2048]{1,2,0:T(8,128)(2,1)S(1)} dynamic-update-slice(bf16[2,64,2048]{1,2,0:T(8,128)(2,1)S(1)} %dynamic_update_slice.49, bf16[2,4,2048]{1,2,0:T(8,128)(2,1)S(1)} %copy.53, s32[]{:T(128)} %constant.99.clone.1, s32[]{:T(128)S(6)} %select_n.115, s32[]{:T(128)} %constant.99.clone.1) | dynamic-update-slice | bytes 65540 | tf_op jit(solution)/shard_map/dynamic_update_slice | solution.py:130
  61.4 7.4 %dynamic_update_slice.51 = bf16[2,64,2048]{1,2,0:T(8,128)(2,1)S(1)} dynamic-update-slice(bf16[2,64,2048]{1,2,0:T(8,128)(2,1)S(1)} %dynamic_update_slice.50, bf16[2,4,2048]{1,2,0:T(8,128)(2,1)S(1)} %copy.54, s32[]{:T(128)} %constant.99.clone.1, s32[]{:T(128)S(6)} %select_n.117, s32[]{:T(128)} %constant.99.clone.1) | dynamic-update-slice | bytes 65540 | tf_op jit(solution)/shard_map/dynamic_update_slice | solution.py:125
  69.3 7.4 %dynamic_update_slice.52 = bf16[2,64,2048]{1,2,0:T(8,128)(2,1)S(1)} dynamic-update-slice(bf16[2,64,2048]{1,2,0:T(8,128)(2,1)S(1)} %dynamic_update_slice.51, bf16[2,4,2048]{1,2,0:T(8,128)(2,1)S(1)} %copy.55, s32[]{:T(128)} %constant.99.clone.1, s32[]{:T(128)S(6)} %select_n.119, s32[]{:T(128)} %constant.99.clone.1) | dynamic-update-slice | bytes 65540 | tf_op jit(solution)/shard_map/dynamic_update_slice | solution.py:130
  77.2 7.4 %dynamic_update_slice.53 = bf16[2,64,2048]{1,2,0:T(8,128)(2,1)S(1)} dynamic-update-slice(bf16[2,64,2048]{1,2,0:T(8,128)(2,1)S(1)} %dynamic_update_slice.52, bf16[2,4,2048]{1,2,0:T(8,128)(2,1)S(1)} %copy.56, s32[]{:T(128)} %constant.99.clone.1, s32[]{:T(128)S(6)} %select_n.121, s32[]{:T(128)} %constant.99.clone.1) | dynamic-update-slice | bytes 65540 | tf_op jit(solution)/shard_map/dynamic_update_slice | solution.py:125
  85.1 7.4 %dynamic_update_slice.54 = bf16[2,64,2048]{1,2,0:T(8,128)(2,1)S(1)} dynamic-update-slice(bf16[2,64,2048]{1,2,0:T(8,128)(2,1)S(1)} %dynamic_update_slice.53, bf16[2,4,2048]{1,2,0:T(8,128)(2,1)S(1)} %copy.57, s32[]{:T(128)} %constant.99.clone.1, s32[]{:T(128)S(6)} %select_n.123, s32[]{:T(128)} %constant.99.clone.1) | dynamic-update-slice | bytes 65540 | tf_op jit(solution)/shard_map/dynamic_update_slice | solution.py:130
  93.1 7.4 %dynamic_update_slice.55 = bf16[2,64,2048]{1,2,0:T(8,128)(2,1)S(1)} dynamic-update-slice(bf16[2,64,2048]{1,2,0:T(8,128)(2,1)S(1)} %dynamic_update_slice.54, bf16[2,4,2048]{1,2,0:T(8,128)(2,1)S(1)} %copy.58, s32[]{:T(128)} %constant.99.clone.1, s32[]{:T(128)S(6)} %select_n.125, s32[]{:T(128)} %constant.99.clone.1) | dynamic-update-slice | bytes 65540 | tf_op jit(solution)/shard_map/dynamic_update_slice | solution.py:125
  101.0 7.4 %dynamic_update_slice.56 = bf16[2,64,2048]{1,2,0:T(8,128)(2,1)S(1)} dynamic-update-slice(bf16[2,64,2048]{1,2,0:T(8,128)(2,1)S(1)} %dynamic_update_slice.55, bf16[2,4,2048]{1,2,0:T(8,128)(2,1)S(1)} %copy.59, s32[]{:T(128)} %constant.99.clone.1, s32[]{:T(128)S(6)} %select_n.127, s32[]{:T(128)} %constant.99.clone.1) | dynamic-update-slice | bytes 65540 | tf_op jit(solution)/shard_map/dynamic_update_slice | solution.py:130
  108.9 7.4 %dynamic_update_slice.57 = bf16[2,64,2048]{1,2,0:T(8,128)(2,1)S(1)} dynamic-update-slice(bf16[2,64,2048]{1,2,0:T(8,128)(2,1)S(1)} %dynamic_update_slice.56, bf16[2,4,2048]{1,2,0:T(8,128)(2,1)S(1)} %copy.60, s32[]{:T(128)} %constant.99.clone.1, s32[]{:T(128)S(6)} %select_n.129, s32[]{:T(128)} %constant.99.clone.1) | dynamic-update-slice | bytes 65540 | tf_op jit(solution)/shard_map/dynamic_update_slice | solution.py:125
  116.9 7.6 %dynamic_update_slice.58 = bf16[2,64,2048]{1,2,0:T(8,128)(2,1)S(1)} dynamic-update-slice(bf16[2,64,2048]{1,2,0:T(8,128)(2,1)S(1)} %dynamic_update_slice.57, bf16[2,4,2048]{1,2,0:T(8,128)(2,1)S(1)} %copy.61, s32[]{:T(128)} %constant.99.clone.1, s32[]{:T(128)S(6)} %select_n.131, s32[]{:T(128)} %constant.99.clone.1) | dynamic-update-slice | bytes 65540 | tf_op jit(solution)/shard_map/dynamic_update_slice | solution.py:130
  125.0 7.4 %dynamic_update_slice.59 = bf16[2,64,2048]{1,2,0:T(8,128)(2,1)S(1)} dynamic-update-slice(bf16[2,64,2048]{1,2,0:T(8,128)(2,1)S(1)} %dynamic_update_slice.58, bf16[2,4,2048]{1,2,0:T(8,128)(2,1)S(1)} %copy.62, s32[]{:T(128)} %constant.99.clone.1, s32[]{:T(128)S(6)} %select_n.133, s32[]{:T(128)} %constant.99.clone.1) | dynamic-update-slice | bytes 65540 | tf_op jit(solution)/shard_map/dynamic_update_slice | solution.py:125
  132.9 7.4 %dynamic_update_slice.60 = bf16[2,64,2048]{1,2,0:T(8,128)(2,1)S(1)} dynamic-update-slice(bf16[2,64,2048]{1,2,0:T(8,128)(2,1)S(1)} %dynamic_update_slice.59, bf16[2,4,2048]{1,2,0:T(8,128)(2,1)S(1)} %copy.63, s32[]{:T(128)} %constant.99.clone.1, s32[]{:T(128)S(6)} %select_n.135, s32[]{:T(128)} %constant.99.clone.1) | dynamic-update-slice | bytes 65540 | tf_op jit(solution)/shard_map/dynamic_update_slice | solution.py:130
  140.9 7.4 %dynamic_update_slice.61 = bf16[2,64,2048]{1,2,0:T(8,128)(2,1)S(1)} dynamic-update-slice(bf16[2,64,2048]{1,2,0:T(8,128)(2,1)S(1)} %dynamic_update_slice.60, bf16[2,4,2048]{1,2,0:T(8,128)(2,1)S(1)} %copy.64, s32[]{:T(128)} %constant.99.clone.1, s32[]{:T(128)S(6)} %select_n.137, s32[]{:T(128)} %constant.99.clone.1) | dynamic-update-slice | bytes 65540 | tf_op jit(solution)/shard_map/dynamic_update_slice | solution.py:125
  148.3 1.3 copy.65
  149.6 7.4 %dynamic_update_slice.62 = bf16[2,64,2048]{1,2,0:T(8,128)(2,1)S(1)} dynamic-update-slice(bf16[2,64,2048]{1,2,0:T(8,128)(2,1)S(1)} %dynamic_update_slice.61, bf16[2,4,2048]{1,2,0:T(8,128)(2,1)S(1)} %copy.65, s32[]{:T(128)} %constant.99.clone.1, s32[]{:T(128)S(6)} %select_n.139, s32[]{:T(128)} %constant.99.clone.1) | dynamic-update-slice | bytes 65540 | tf_op jit(solution)/shard_map/dynamic_update_slice | solution.py:130
  157.0 2.2 copy.66
  159.2 11.4 %dynamic_update_slice.63 = bf16[2,64,2048]{1,2,0:T(8,128)(2,1)S(1)} dynamic-update-slice(bf16[2,64,2048]{1,2,0:T(8,128)(2,1)S(1)} %dynamic_update_slice.62, bf16[2,4,2048]{1,2,0:T(8,128)(2,1)} %copy.66, s32[]{:T(128)} %constant.99.clone.1, s32[]{:T(128)S(6)} %select_n.141, s32[]{:T(128)} %constant.99.clone.1) | dynamic-update-slice | bytes 65540 | tf_op jit(solution)/shard_map/dynamic_update_slice | solution.py:125
  170.6 2.2 multiply_reduce_fusion
  174.2 40.6 %all_to_all.20 = bf16[16,16,2048]{2,1,0:T(8,128)(2,1)S(1)} all-to-all(bf16[16,16,2048]{2,1,0:T(8,128)(2,1)S(1)} %broadcast_in_dim.4), channel_id=1, replica_groups=mesh['sp_0'=8,'sp_1'=4,'tp'=16] {'tp'}, dimensions={0} | all-to-all | bytes 2097152 | tf_op jit(solution)/shard_map/all_to_all | solution.py:16
  214.8 1.7 convolution_convert_fusion.5
  216.4 46.2 %all-gather.2.cloned.1.call-done = bf16[2048,1,514]{2,0,1:T(8,128)(2,1)} async-done(((bf16[64,1,514]{2,0,1:T(8,128)(2,1)}), bf16[2048,1,514]{2,0,1:T(8,128)(2,1)}) %all-gather.2.cloned.1.call-update) | async-done | bytes 2105360 | tf_op jit(solution)/shard_map/all_gather | solution.py:35
  262.6 1.9 convert_reduce_fusion.1
  264.5 3.1 fusion.3
  267.6 3.3 fusion.5
  270.9 1.5 fusion.6
  272.4 4.0 fusion.8
  276.3 5.0 %fusion.4 = bf16[256,2048]{1,0:T(8,128)(2,1)} fusion(f32[256,2048]{1,0:T(8,128)} %fusion.8, bf16[2048,256]{1,0:T(8,128)(2,1)S(1)} %copy-done, f32[2048,256]{1,0:T(8,128)} %fusion.3, bf16[2048,1,514]{2,0,1:T(8,128)(2,1)} %all-gather.2.cloned.1.call-done), kind=kOutput, calls=%fused_computation.7 | convolution fusion | flops 538509312 | bytes 7340032 | tf_op jit(solution)/shard_map/dot_general | solution.py:65
  281.3 11.8 %all-to-all-start.2 = ((bf16[16,16,2048]{2,1,0:T(8,128)(2,1)}), bf16[16,16,2048]{2,1,0:T(8,128)(2,1)}, u32[]{:S(2)}, u32[]{:S(2)}) async-start(bf16[16,16,2048]{2,1,0:T(8,128)(2,1)} %bitcast.20), calls=%async_computation.3 | async-start | bytes 2097152 | tf_op jit(solution)/shard_map/all_to_all | solution.py:54
  293.1 19.5 %reduce-scatter.5.cloned.1.call-done = bf16[256,1,256]{0,2,1:T(8,128)(2,1)} async-done(((bf16[2048,1,256]{0,2,1:T(8,128)(2,1)}), bf16[256,1,256]{0,2,1:T(8,128)(2,1)}) %reduce-scatter.5.cloned.1.call-update) | async-done | bytes 131088 | tf_op jit(solution)/shard_map/reduce_scatter | solution.py:43
  312.6 1.7 copy.74
  314.3 26.3 %reduce-scatter.7.cloned.1.call-done = bf16[64,256]{1,0:T(8,128)(2,1)} async-done(((bf16[256,256]{1,0:T(8,128)(2,1)}), bf16[64,256]{1,0:T(8,128)(2,1)}) %reduce-scatter.7.cloned.1.call-update) | async-done | bytes 32784 | tf_op jit(solution)/shard_map/reshape | solution.py:178
  340.6 1.3 convolution_convert_fusion.1
  342.7 9.5 %all-to-all-start.1 = ((bf16[16,4,2048]{2,1,0:T(4,128)(2,1)}), bf16[16,4,2048]{2,1,0:T(4,128)(2,1)S(1)}, u32[]{:S(2)}, u32[]{:S(2)}) async-start(bf16[16,4,2048]{2,1,0:T(4,128)(2,1)} %reshape.145), calls=%async_computation.2 | async-start | bytes 524288 | tf_op jit(solution)/shard_map/all_to_all | solution.py:54
  352.2 1.7 fusion.20
  353.9 9.8 %all-to-all-done.1 = bf16[16,4,2048]{2,1,0:T(4,128)(2,1)S(1)} async-done(((bf16[16,4,2048]{2,1,0:T(4,128)(2,1)}), bf16[16,4,2048]{2,1,0:T(4,128)(2,1)S(1)}, u32[]{:S(2)}, u32[]{:S(2)}) %all-to-all-start.1) | async-done | bytes 262176 | tf_op jit(solution)/shard_map/all_to_all | solution.py:54
  363.7 10.3 %all-to-all-start.3 = ((f32[32,64,256]{2,1,0:T(8,128)}), f32[32,64,256]{2,1,0:T(8,128)S(1)}, u32[]{:S(2)}, u32[]{:S(2)}) async-start(f32[32,64,256]{2,1,0:T(8,128)} %fusion.20), calls=%async_computation.4 | async-start | bytes 4194304 | tf_op jit(solution)/shard_map/all_to_all | solution.py:60
  374.0 2.0 convert_reduce_fusion
  377.0 48.7 %all-to-all-done.3 = f32[32,64,256]{2,1,0:T(8,128)S(1)} async-done(((f32[32,64,256]{2,1,0:T(8,128)}), f32[32,64,256]{2,1,0:T(8,128)S(1)}, u32[]{:S(2)}, u32[]{:S(2)}) %all-to-all-start.3) | async-done | bytes 2097184 | tf_op jit(solution)/shard_map/all_to_all | solution.py:60
  (88 shorter events, 22.2 us)
Async XLA Ops:
  7.2 260.4 %copy-start = (bf16[2048,256]{1,0:T(8,128)(2,1)S(1)}, bf16[2048,256]{1,0:T(8,128)(2,1)}, u32[]{:S(2)}) copy-start(bf16[2048,256]{1,0:T(8,128)(2,1)} %param.15) | copy-start | bytes 3145732
  7.2 255.4 %all-gather.2.cloned.1.call-start = ((), (), s32[]{:S(2)}) async-start(), calls=%async_computation.6 | async-start | bytes 2703360 | tf_op jit(solution)/shard_map/all_gather | solution.py:35
  10.4 2.9 collective-permute-start
  12.3 3.3 collective-permute-start.1
  13.3 3.3 collective-permute-start.2
  15.6 3.6 collective-permute-start.3
  16.6 4.3 collective-permute-start.4
  19.3 3.3 collective-permute-start.5
  20.9 4.6 %collective-permute-start.6 = (bf16[2,4,2048]{2,1,0:T(4,128)(2,1)S(1)}, bf16[2,4,2048]{2,1,0:T(4,128)(2,1)S(1)}, u32[]{:S(2)}, u32[]{:S(2)}) collective-permute-start(bf16[2,4,2048]{2,1,0:T(4,128)(2,1)S(1)} %collective-permute-done.4), channel_id=1, source_target_pairs={{0,1},{1,2},{2,3},{3,4},{4,5},{5,6},{6,7},{7,8},{8,9},{9,10},{10,1... | collective-permute-start | bytes 98312 | tf_op jit(solution)/shard_map/ppermute | solution.py:124
  22.6 3.3 collective-permute-start.7
  25.4 4.6 %collective-permute-start.8 = (bf16[2,4,2048]{2,1,0:T(4,128)(2,1)S(1)}, bf16[2,4,2048]{2,1,0:T(4,128)(2,1)S(1)}, u32[]{:S(2)}, u32[]{:S(2)}) collective-permute-start(bf16[2,4,2048]{2,1,0:T(4,128)(2,1)S(1)} %collective-permute-done.6), channel_id=1, source_target_pairs={{0,1},{1,2},{2,3},{3,4},{4,5},{5,6},{6,7},{7,8},{8,9},{9,10},{10,1... | collective-permute-start | bytes 98312 | tf_op jit(solution)/shard_map/ppermute | solution.py:124
  25.9 4.2 collective-permute-start.9
  30.0 4.6 %collective-permute-start.10 = (bf16[2,4,2048]{2,1,0:T(4,128)(2,1)S(1)}, bf16[2,4,2048]{2,1,0:T(4,128)(2,1)S(1)}, u32[]{:S(2)}, u32[]{:S(2)}) collective-permute-start(bf16[2,4,2048]{2,1,0:T(4,128)(2,1)S(1)} %collective-permute-done.8), channel_id=1, source_target_pairs={{0,1},{1,2},{2,3},{3,4},{4,5},{5,6},{6,7},{7,8},{8,9},{9,10},{10,1... | collective-permute-start | bytes 98312 | tf_op jit(solution)/shard_map/ppermute | solution.py:124
  30.2 10.6 %copy-start.10 = (bf16[2,4,2048]{2,1,0:T(4,128)(2,1)}, bf16[2,4,2048]{2,1,0:T(4,128)(2,1)S(1)}, u32[]{:S(2)}) copy-start(bf16[2,4,2048]{2,1,0:T(4,128)(2,1)S(1)} %collective-permute-done.9) | copy-start | bytes 98308
  30.2 4.6 %collective-permute-start.11 = (bf16[2,4,2048]{2,1,0:T(4,128)(2,1)S(1)}, bf16[2,4,2048]{2,1,0:T(4,128)(2,1)S(1)}, u32[]{:S(2)}, u32[]{:S(2)}) collective-permute-start(bf16[2,4,2048]{2,1,0:T(4,128)(2,1)S(1)} %collective-permute-done.9), channel_id=1, source_target_pairs={{0,15},{1,0},{2,1},{3,2},{4,3},{5,4},{6,5},{7,6},{8,7},{9,8},{10,9... | collective-permute-start | bytes 98312 | tf_op jit(solution)/shard_map/ppermute | solution.py:129
  34.5 6.2 %copy-start.12 = (bf16[2,4,2048]{2,1,0:T(4,128)(2,1)}, bf16[2,4,2048]{2,1,0:T(4,128)(2,1)S(1)}, u32[]{:S(2)}) copy-start(bf16[2,4,2048]{2,1,0:T(4,128)(2,1)S(1)} %collective-permute-done.10) | copy-start | bytes 98308
  34.6 4.6 %collective-permute-start.12 = (bf16[2,4,2048]{2,1,0:T(4,128)(2,1)S(1)}, bf16[2,4,2048]{2,1,0:T(4,128)(2,1)S(1)}, u32[]{:S(2)}, u32[]{:S(2)}) collective-permute-start(bf16[2,4,2048]{2,1,0:T(4,128)(2,1)S(1)} %collective-permute-done.10), channel_id=1, source_target_pairs={{0,1},{1,2},{2,3},{3,4},{4,5},{5,6},{6,7},{7,8},{8,9},{9,10},{10,1... | collective-permute-start | bytes 98312 | tf_op jit(solution)/shard_map/ppermute | solution.py:124
  34.7 113.6 %collective-permute-start.13 = (bf16[2,4,2048]{2,1,0:T(4,128)(2,1)S(1)}, bf16[2,4,2048]{2,1,0:T(4,128)(2,1)}, u32[]{:S(2)}, u32[]{:S(2)}) collective-permute-start(bf16[2,4,2048]{2,1,0:T(4,128)(2,1)S(1)} %collective-permute-done.11), channel_id=1, source_target_pairs={{0,15},{1,0},{2,1},{3,2},{4,3},{5,4},{6,5},{7,6},{8,7},{9,8},{10,9... | collective-permute-start | bytes 98312 | tf_op jit(solution)/shard_map/ppermute | solution.py:129
  39.1 117.9 %collective-permute-start.14 = (bf16[2,4,2048]{2,1,0:T(4,128)(2,1)S(1)}, bf16[2,4,2048]{2,1,0:T(4,128)(2,1)}, u32[]{:S(2)}, u32[]{:S(2)}) collective-permute-start(bf16[2,4,2048]{2,1,0:T(4,128)(2,1)S(1)} %collective-permute-done.12), channel_id=1, source_target_pairs={{0,1},{1,2},{2,3},{3,4},{4,5},{5,6},{6,7},{7,8},{8,9},{9,10},{10,1... | collective-permute-start | bytes 98312 | tf_op jit(solution)/shard_map/ppermute | solution.py:124
  108.4 7.9 %copy-start.11 = (bf16[2,4,2048]{2,1,0:T(4,128)(2,1)S(1)}, bf16[2,4,2048]{2,1,0:T(4,128)(2,1)}, u32[]{:S(2)}) copy-start(bf16[2,4,2048]{2,1,0:T(4,128)(2,1)} %copy-done.10) | copy-start | bytes 98308
  116.4 8.1 %copy-start.13 = (bf16[2,4,2048]{2,1,0:T(4,128)(2,1)S(1)}, bf16[2,4,2048]{2,1,0:T(4,128)(2,1)}, u32[]{:S(2)}) copy-start(bf16[2,4,2048]{2,1,0:T(4,128)(2,1)} %copy-done.12) | copy-start | bytes 98308
  157.0 13.6 %copy-start.9 = (bf16[64,256]{1,0:T(8,128)(2,1)S(1)}, bf16[64,256]{1,0:T(8,128)(2,1)}, u32[]{:S(2)}) copy-start(bf16[64,256]{1,0:T(8,128)(2,1)} %param.17) | copy-start | bytes 98308
  159.2 13.7 %copy-start.4 = (bf16[2048,256]{1,0:T(8,128)(2,1)S(1)}, bf16[2048,256]{1,0:T(8,128)(2,1)}, u32[]{:S(2)}) copy-start(bf16[2048,256]{1,0:T(8,128)(2,1)} %param.13) | copy-start | bytes 3145732
  170.6 3.6 copy-start.1
  170.6 3.5 copy-start.8
  174.0 138.7 %reduce-scatter.5.cloned.1.call-start = ((), (), s32[]{:S(2)}) async-start(), calls=%async_computation.7 | async-start | bytes 1179648 | tf_op jit(solution)/shard_map/reduce_scatter | solution.py:43
  270.9 1.5 copy-start.3
  281.3 59.3 %copy-start.5 = (bf16[2048,256]{1,0:T(8,128)(2,1)S(1)}, bf16[2048,256]{1,0:T(8,128)(2,1)}, u32[]{:S(2)}) copy-start(bf16[2048,256]{1,0:T(8,128)(2,1)} %param.13) | copy-start | bytes 3145732
  281.3 70.8 %copy-start.2 = (bf16[2,64,2048]{1,2,0:T(8,128)(2,1)S(1)}, bf16[2,64,2048]{1,2,0:T(8,128)(2,1)}, u32[]{:S(2)}) copy-start(bf16[2,64,2048]{1,2,0:T(8,128)(2,1)} %copy-done.1) | copy-start | bytes 1572868
  281.3 61.3 %all-to-all-start.2 = ((bf16[16,16,2048]{2,1,0:T(8,128)(2,1)}), bf16[16,16,2048]{2,1,0:T(8,128)(2,1)}, u32[]{:S(2)}, u32[]{:S(2)}) async-start(bf16[16,16,2048]{2,1,0:T(8,128)(2,1)} %bitcast.20), calls=%async_computation.3 | async-start | bytes 2097152 | tf_op jit(solution)/shard_map/all_to_all | solution.py:54
  293.1 47.5 %reduce-scatter.7.cloned.1.call-start = ((), (), s32[]{:S(2)}) async-start(), calls=%async_computation.8 | async-start | bytes 163840 | tf_op jit(solution)/shard_map/reshape | solution.py:178
  340.6 11.6 %copy-start.7 = (bf16[64,256]{1,0:T(8,128)(2,1)S(1)}, bf16[64,256]{1,0:T(8,128)(2,1)}, u32[]{:S(2)}) copy-start(bf16[64,256]{1,0:T(8,128)(2,1)} %reduce-scatter.7.cloned.1.call-done) | copy-start | bytes 98308
  342.7 21.1 %all-to-all-start.1 = ((bf16[16,4,2048]{2,1,0:T(4,128)(2,1)}), bf16[16,4,2048]{2,1,0:T(4,128)(2,1)S(1)}, u32[]{:S(2)}, u32[]{:S(2)}) async-start(bf16[16,4,2048]{2,1,0:T(4,128)(2,1)} %reshape.145), calls=%async_computation.2 | async-start | bytes 524288 | tf_op jit(solution)/shard_map/all_to_all | solution.py:54
  353.9 22.2 %copy-start.6 = (bf16[4,2048]{1,0:T(4,128)(2,1)S(1)}, bf16[4,2048]{1,0:T(4,128)(2,1)}, u32[]{:S(2)}) copy-start(bf16[4,2048]{1,0:T(4,128)(2,1)} %param.10) | copy-start | bytes 49156
  363.7 62.0 %all-to-all-start.3 = ((f32[32,64,256]{2,1,0:T(8,128)}), f32[32,64,256]{2,1,0:T(8,128)S(1)}, u32[]{:S(2)}, u32[]{:S(2)}) async-start(f32[32,64,256]{2,1,0:T(8,128)} %fusion.20), calls=%async_computation.4 | async-start | bytes 4194304 | tf_op jit(solution)/shard_map/all_to_all | solution.py:60
Sparse Core Ops, SparseCore 0:
  174.1 88.4 all-gather.1
  272.5 40.1 reduce-scatter.4
  316.0 24.5 reduce-scatter.6
